TPU v7x, 512 devices: a whole 4x8x8 slice. The times are simulated.
512 devices in a mesh: sp: 32 (over z, x), dp: 16 (over y, core).
Axes of the slice: x: 4, y: 8, z: 8, core: 2. Of those that a mesh axis runs over, the one named last changes fastest.
Arguments:
- tokens: bfloat16 [16, 16384, 2048], P('dp', 'sp'), may hold values from -6 to 6
- segments: int32 [16, 16384], P('dp', 'sp'), may hold values from 0 to 15, never falling along the last dimension, each value on 1 to 2048 neighbouring positions
- w_lin: bfloat16 [2048, 1024], P('dp'), may hold values from -0.125 to 0.125
- w_gate: bfloat16 [2048, 1024], P('dp'), may hold values from -0.125 to 0.125
- w_out: bfloat16 [1024, 2048], P(None, 'dp'), may hold values from -0.1875 to 0.1875
- conv_kernel: float32 [31, 1024], replicated, may hold values from -1 to 1
- conv_bias: float32 [1024], replicated, may hold values from -3 to 3
- norm_gain: float32 [1024], replicated, may hold values from 0.1 to 1.9
- norm_bias: float32 [1024], replicated, may hold values from -3 to 3
Outputs:
- mixed_out: bfloat16 [16, 16384, 2048], P('dp', 'sp')
Inputs may be any that keep to these rules, and one draw needn't show every extreme that they name: `segments`: within each sequence document numbers never fall; a document is a run of equal numbers of at most four times 512 positions.
All inputs are finite; a program needn't handle non-finite values.
Results may differ from a plain program's by a relative error of at most 0.0062.
Values may be sent and summed in bfloat16 or wider, within the bound.
A program may use at most 64 MiB of HBM per device.

v0:
```python
import jax
import jax.numpy as jnp
from jax import lax
from jax.sharding import PartitionSpec as P

K = 31


def sent_together(arrays, axis, dim, along):
    both = jnp.concatenate(arrays, axis=along)
    result, at, outs = (lax.all_gather(both, axis, axis=dim, tiled=True), 0, [])
    for a in arrays:
        outs.append(lax.slice_in_dim(result, at, at + a.shape[along], axis=along))
        at += a.shape[along]
    return tuple(outs)


def from_behind(value, axis, by):
    devices = lax.axis_size(axis)
    pairs = [(i, i + by) for i in range(devices) if 0 <= i + by < devices]
    return lax.ppermute(value, axis, pairs)


def conv_doc(values, doc_ids, kernel, bias):
    taps = kernel.shape[0]
    reach = taps - 1
    length = values.shape[1]
    place = lax.iota(jnp.int32, length)
    change = jnp.concatenate([jnp.ones((1,), jnp.bool_), doc_ids[1:] != doc_ids[:-1]])
    begins = lax.cummax(jnp.where(change, place, 0), axis=0)[reach:]
    here = place[reach:]
    total = bias[:, None] + kernel[reach][:, None] * values[:, reach:].astype(jnp.float32)
    for back in range(1, taps):
        piece = values[:, reach - back : length - back].astype(jnp.float32)
        keep = here - back >= begins
        total = total + kernel[reach - back][:, None] * jnp.where(keep[None, :], piece, 0.0)
    return total


def body(tokens, segments, w_lin, w_gate, w_out, conv_kernel, conv_bias, norm_gain, norm_bias):
    rows = tokens[0]
    doc_ids = segments[0]
    count = rows.shape[0]
    reach = K - 1
    pieces = sent_together((w_lin, w_gate), "dp", 0, 1)
    first = jnp.einsum("rc,tr->ct", pieces[0], rows, preferred_element_type=jnp.float32)
    second = jnp.einsum("rc,tr->ct", pieces[1], rows, preferred_element_type=jnp.float32)
    glu = (first * jax.nn.sigmoid(second)).astype(jnp.bfloat16)
    tail, tail_ids = from_behind((glu[:, count - reach :], doc_ids[count - reach :]), "sp", 1)
    extended = jnp.concatenate([tail, glu], axis=1)
    ext_ids = jnp.concatenate([tail_ids, doc_ids], axis=0)
    conv = conv_doc(extended, ext_ids, conv_kernel, conv_bias)
    conved = lax.optimization_barrier(conv.astype(jnp.bfloat16))
    values = conved.astype(jnp.float32)
    mean = jnp.mean(values, axis=0, keepdims=True)
    var = jnp.mean(jnp.square(values - mean), axis=0, keepdims=True)
    normed = (values - mean) * lax.rsqrt(var + 1e-05) * norm_gain[:, None] + norm_bias[:, None]
    act = jax.nn.silu(normed).astype(jnp.bfloat16)
    mixed_out = jnp.einsum(
        "ct,cr->tr",
        act,
        lax.all_gather(w_out, "dp", axis=1, tiled=True),
        preferred_element_type=jnp.float32,
    ).astype(jnp.bfloat16)
    return mixed_out[None]


def solution(mesh):
    placed = (
        P("dp", "sp", None),
        P("dp", "sp"),
        P("dp", None),
        P("dp", None),
        P(None, "dp"),
        P(),
        P(),
        P(),
        P(),
    )
    return jax.shard_map(
        body, mesh=mesh, in_specs=placed, out_specs=P("dp", "sp", None), check_vma=False
    )
```

profile of v0, /device:TPU:1, one launch (start us, length us, event | category | flops | bytes accessed | tf_op | source)
XLA Modules:
  0.0 140.4 jit_solution(699867994584362061)
XLA Ops:
  6.5 2.0 %pad_maximum_fusion.1 = bf16[128,2048]{1,0:T(8,128)(2,1)} fusion(bf16[128,1024]{1,0:T(8,128)(2,1)} %param.12, bf16[128,1024]{1,0:T(8,128)(2,1)} %param.11), kind=kLoop, calls=%fused_computation.92 | loop fusion | flops 1048576 | bytes 1048576 | tf_op jit(solution)/shard_map/concatenate | solution.py:10
  8.6 0.7 all-gather.5.cloned.1.call-update
  9.3 0.7 slice_bitcast_fusion
  10.1 3.9 %collective-permute-start = (s32[30]{0:T(128)S(1)}, s32[30]{0:T(128)S(1)}, u32[]{:S(2)}, u32[]{:S(2)}) collective-permute-start(s32[30]{0:T(128)S(1)} %slice_bitcast_fusion), channel_id=1, source_target_pairs={{0,16},{16,32},{32,48},{48,64},{64,80},{80,96},{96,112},{112,128},... | collective-permute-start | bytes 368 | tf_op jit(solution)/shard_map/ppermute | solution.py:21
  14.0 1.4 fusion.58
  15.4 1.1 fusion.59
  16.6 0.1 slice_compare_fusion
  16.7 0.1 iota_select_fusion
  16.8 0.3 reduce-window.9
  17.1 0.1 slice_reduce_fusion
  17.3 0.1 add_compare_fusion.29
  17.4 0.1 add_compare_fusion.20
  17.5 0.1 add_compare_fusion.11
  17.6 55.9 %all-gather.3.cloned.1.call-done = bf16[2048,2048]{1,0:T(8,128)(2,1)} async-done(((bf16[128,2048]{1,0:T(8,128)(2,1)}), bf16[2048,2048]{1,0:T(8,128)(2,1)}) %all-gather.3.cloned.1.call-update) | async-done | bytes 8388624 | tf_op jit(solution)/shard_map/all_gather | solution.py:11
  73.5 4.7 %fusion = f32[1024,512]{0,1:T(8,128)S(1)} fusion(bf16[2048,2048]{1,0:T(8,128)(2,1)} %all-gather.3.cloned.1.call-done, bf16[1,512,2048]{2,1,0:T(8,128)(2,1)S(1)} %copy-done), kind=kOutput, calls=%fused_computation.29 | convolution fusion | flops 2147483648 | bytes 8388608 | tf_op jit(solution)/shard_map/rc,tr->ct/dot_general | solution.py:47
  78.2 2.5 %multiply_convert_fusion = bf16[1024,512]{0,1:T(8,128)(2,1)S(1)} fusion(f32[1024,512]{0,1:T(8,128)S(1)} %fusion, bf16[2048,2048]{1,0:T(8,128)(2,1)S(1)} %copy-done.3, bf16[1,512,2048]{2,1,0:T(8,128)(2,1)S(1)} %copy-done), kind=kOutput, calls=%fused_computation.51 | convolution fusion | flops 2150105088 | bytes 9437184 | tf_op jit(solution)/shard_map/rc,tr->ct/dot_general | solution.py:46
  80.7 3.1 %collective-permute-start.1 = (bf16[1024,30]{0,1:T(8,128)(2,1)S(1)}, bf16[1024,30]{0,1:T(8,128)(2,1)S(1)}, u32[]{:S(2)}, u32[]{:S(2)}) collective-permute-start(bf16[1024,30]{0,1:T(8,128)(2,1)S(1)} %slice.351), channel_id=1, source_target_pairs={{0,16},{16,32},{32,48},{48,64},{64,80},{80,96},{96,112},{112,128},... | collective-permute-start | bytes 184328 | tf_op jit(solution)/shard_map/ppermute | solution.py:21
  83.8 0.1 add_compare_fusion.2
  83.9 1.2 collective-permute-done.1
  85.2 15.9 %add_convert_fusion = bf16[1024,512]{0,1:T(8,128)(2,1)S(1)} fusion(bf16[1024,512]{0,1:T(8,128)(2,1)S(1)} %multiply_convert_fusion, bf16[1024,30]{0,1:T(8,128)(2,1)S(1)} %collective-permute-done.1, f32[1024]{0:T(1024)S(1)} %bitcast.77, f32[1024]{0:T(1024)S(1)} %bitcast.78, f32[1024]{0:T(1024)S(1)} %bitcast.49, f32[1024]{0:T(1024)S(1)} %bitcast.50, ...), kind=kLoop, calls=%fused_computation.50 | loop fusion | flops 112197632 | bytes 2305024 | tf_op jit(solution)/shard_map/convert_element_type | solution.py:53
  101.0 0.2 convert_reduce_fusion
  101.3 0.4 fusion.7
  101.7 25.5 %all-gather.5.cloned.1.call-done = bf16[1024,2048]{1,0:T(8,128)(2,1)} async-done(((bf16[1024,128]{1,0:T(8,128)(2,1)}), bf16[1024,2048]{1,0:T(8,128)(2,1)}) %all-gather.5.cloned.1.call-update) | async-done | bytes 4194320 | tf_op jit(solution)/shard_map/all_gather | solution.py:62
  127.2 6.4 %fusion.4 = bf16[1,512,2048]{2,1,0:T(8,128)(2,1)} fusion(bf16[1024,2048]{1,0:T(8,128)(2,1)} %all-gather.5.cloned.1.call-done, bf16[1024,512]{0,1:T(8,128)(2,1)S(1)} %add_convert_fusion, f32[1024]{0:T(1024)S(1)} %copy-done.4, f32[1024]{0:T(1024)S(1)} %copy-done.5, f32[512]{0:T(512)S(1)} %add_rsqrt_fusion, f32[512]{0:T(512)S(1)} %broadcast_multiply_fusion), kind=kOutput, calls=%fused_computation.34 | convolution fusion | flops 2153775104 | bytes 7352320 | tf_op jit(solution)/shard_map/ct,cr->tr/dot_general | solution.py:59
  (25 shorter events, 0.4 us)
Async XLA Ops:
  6.5 67.0 %copy-start = (bf16[1,512,2048]{2,1,0:T(8,128)(2,1)S(1)}, bf16[1,512,2048]{2,1,0:T(8,128)(2,1)}, u32[]{:S(2)}) copy-start(bf16[1,512,2048]{2,1,0:T(8,128)(2,1)} %param.9) | copy-start | bytes 6291460
  6.5 10.0 %copy-start.2 = (s32[1,512]{1,0:T(1,128)S(1)}, s32[1,512]{1,0:T(1,128)}, u32[]{:S(2)}) copy-start(s32[1,512]{1,0:T(1,128)} %param.10) | copy-start | bytes 6148
  6.5 67.0 %all-gather.3.cloned.1.call-start = ((), (), s32[]{:S(2)}) async-start(), calls=%async_computation | async-start | bytes 8912896 | tf_op jit(solution)/shard_map/all_gather | solution.py:11
  8.6 118.6 %all-gather.5.cloned.1.call-start = ((), (), s32[]{:S(2)}) async-start(), calls=%async_computation.1 | async-start | bytes 4456448 | tf_op jit(solution)/shard_map/all_gather | solution.py:62
  10.1 6.4 %collective-permute-start = (s32[30]{0:T(128)S(1)}, s32[30]{0:T(128)S(1)}, u32[]{:S(2)}, u32[]{:S(2)}) collective-permute-start(s32[30]{0:T(128)S(1)} %slice_bitcast_fusion), channel_id=1, source_target_pairs={{0,16},{16,32},{32,48},{48,64},{64,80},{80,96},{96,112},{112,128},... | collective-permute-start | bytes 368 | tf_op jit(solution)/shard_map/ppermute | solution.py:21
  73.5 4.7 %copy-start.3 = (bf16[2048,2048]{1,0:T(8,128)(2,1)S(1)}, bf16[2048,2048]{1,0:T(8,128)(2,1)}, u32[]{:S(2)}) copy-start(bf16[2048,2048]{1,0:T(8,128)(2,1)} %all-gather.3.cloned.1.call-done) | copy-start | bytes 25165828
  78.2 7.0 %copy-start.1 = (f32[1024]{0:T(1024)S(1)}, f32[1024]{0:T(1024)}, u32[]{:S(2)}) copy-start(f32[1024]{0:T(1024)} %param.15) | copy-start | bytes 12292
  80.7 4.4 %collective-permute-start.1 = (bf16[1024,30]{0,1:T(8,128)(2,1)S(1)}, bf16[1024,30]{0,1:T(8,128)(2,1)S(1)}, u32[]{:S(2)}, u32[]{:S(2)}) collective-permute-start(bf16[1024,30]{0,1:T(8,128)(2,1)S(1)} %slice.351), channel_id=1, source_target_pairs={{0,16},{16,32},{32,48},{48,64},{64,80},{80,96},{96,112},{112,128},... | collective-permute-start | bytes 184328 | tf_op jit(solution)/shard_map/ppermute | solution.py:21
  85.2 42.0 %copy-start.4 = (f32[1024]{0:T(1024)S(1)}, f32[1024]{0:T(1024)}, u32[]{:S(2)}) copy-start(f32[1024]{0:T(1024)} %param.17) | copy-start | bytes 12292
  85.2 42.0 %copy-start.5 = (f32[1024]{0:T(1024)S(1)}, f32[1024]{0:T(1024)}, u32[]{:S(2)}) copy-start(f32[1024]{0:T(1024)} %param.16) | copy-start | bytes 12292
Sparse Core Ops, SparseCore 0:
  9.5 64.0 all-gather.2
  75.6 51.5 all-gather.4
where the time goes:
time: 141 us; the launch traced here: 140 us
  waiting for transfers between devices  83.4 us (59%)
  other arithmetic  19.5 us (14%)
  matrix products  13.5 us (10%)
  between operations  13.5 us (10%)
  starting transfers between devices  7.06 us (5%)
  local copies, waits for them, and re-layouts  3.47 us (2%)
    all_gather x1, waiting for transfers between devices, sent_together(): result, at, outs = (lax.all_gather(both, axis, axis=dim, tiled=True), 0, [])  55.9 us
    all_gather x1, waiting for transfers between devices, body(): lax.all_gather(w_out, 'dp', axis=1, tiled=True)  25.5 us
    convert_element_type x1, other arithmetic, body(): conved = lax.optimization_barrier(conv.astype(jnp.bfloat16))  15.9 us
    ppermute x2, starting transfers between devices, from_behind(): return lax.ppermute(value, axis, pairs)  7.01 us
    dot_general x1, matrix products, body(): jnp.einsum('ct,cr->tr', act, lax.all_gather(w_out, 'dp', axis=1, tiled=Tr...  6.35 us
    dot_general x1, matrix products, body(): jnp.einsum('rc,tr->ct', pieces[1], rows, preferred_element_type=jnp.float32)  4.66 us
  transfers between devices with their start and end apart: 4, of which 3 were waited for; matrix products, arithmetic and copies ran while one was open for 20% of the time, Pallas kernels for 0%

commit v1 on v0

v1 whole, which is shorter than its diff:
```python
import functools

import jax
import jax.numpy as jnp
from jax import lax
from jax.experimental import pallas as pl
from jax.experimental.pallas import tpu as pltpu
from jax.sharding import PartitionSpec as P

MESH = pl.DeviceIdType.MESH
F32, BF16 = jnp.float32, jnp.bfloat16
NX, NY, NZ = 4, 8, 8
UNITS, IN_UNITS = 12, 8
TOK, TAIL, ROWS = 512, 32, 544
TAPS = 31
LEAD_SEND, LEAD_FORWARD, LEAD_FAR, LEAD_NEAR_PAIR, LEAD_FAR_PAIR = 5, 3, 2, 2, 1


def offset_of(e):
    return ((e + 1) // 2) * (2 * (e % 2) - 1)


def kernel(
    tok, seg, wl, wg, wo, ck, cb, ng, nb, out,
    w, x, ids, idc, dist, taps, ckv, vecs, g, conv, act, ost,
    load_sem, misc_sem, recv_sem, send_sem,
):
    sp, dp = lax.axis_index("sp"), lax.axis_index("dp")
    px, pz = sp % NX, sp // NX
    py, pc = dp // 2, dp % 2

    def at(dx=0, dy=0, dz=0):
        return (
            ((pz + dz + NZ) % NZ) * NX + (px + dx + NX) % NX,
            ((py + dy + NY) % NY) * 2 + pc,
        )

    after = ((sp + 1) % (NX * NZ), dp)
    before = ((sp + NX * NZ - 1) % (NX * NZ), dp)
    partner = (sp, py * 2 + 1 - pc)

    def local(src, dst, sem):
        pltpu.make_async_copy(src, dst, sem).start()

    def wait(region, sem):
        pltpu.make_async_copy(region, region, sem).wait()

    for u in range(IN_UNITS):
        lanes = pl.ds(128 * u, 128)
        local(wl.at[:, :, lanes], w.at[u, 0, pc, :, :, pl.ds(0, 128)], load_sem.at[u])
        local(wg.at[:, :, lanes], w.at[u, 0, pc, :, :, pl.ds(128, 128)], load_sem.at[u])
    for e in range(8):
        src = pl.multiple_of(256 * ((py + offset_of(e) + NY) % NY), 256)
        local(tok.at[:, pl.ds(src, 256)], x.at[pl.ds(TAIL, TOK), pl.ds(256 * e, 256)], misc_sem.at[0])
    local(seg, ids.at[:, pl.ds(128, TOK)], misc_sem.at[1])
    for u in range(8):
        local(wo.at[u], w.at[8 + u // 2, 0, pc, :, :, pl.ds(128 * (u % 2), 128)], load_sem.at[8 + u // 2])
    local(ck, ckv, misc_sem.at[2])
    local(cb, vecs.at[0], misc_sem.at[3])
    local(ng, vecs.at[1], misc_sem.at[4])
    local(nb, vecs.at[2], misc_sem.at[5])

    barrier = pltpu.get_barrier_semaphore()
    peers = [at(dy=1), at(dy=-1), at(dy=2), at(dy=-2), at(dx=1), at(dx=-1), at(dz=1), at(dz=-1),
             partner, after, before]
    for peer in peers:
        pl.semaphore_signal(barrier, inc=1, device_id=peer, device_id_type=MESH)
    pl.semaphore_wait(barrier, len(peers))

    def send(ref, kind, unit, peer, dst=None):
        pltpu.make_async_remote_copy(
            src_ref=ref, dst_ref=ref if dst is None else dst,
            send_sem=send_sem.at[kind], recv_sem=recv_sem.at[kind, unit],
            device_id=peer, device_id_type=MESH,
        ).start()

    def class_of(parity):
        return (px * (1 + parity) + pz * (2 - parity)) % 4

    def planes(parity):
        def mix(a, b):
            return tuple((1 - parity) * i + parity * j for i, j in zip(a, b))
        return (mix(at(dx=1), at(dz=1)), mix(at(dx=-1), at(dz=-1)),
                mix(at(dz=1), at(dx=1)), mix(at(dz=-1), at(dx=-1)))

    def in_plane(m, first, count, kind):
        parity = m % 2
        q = class_of(parity)
        heavy_up, heavy_down, light_up, light_down = planes(parity)
        span = pl.ds(first, count)
        whole = w.at[m, span, pc, q]
        send(whole, kind, m, heavy_up)
        send(whole, kind, m, heavy_down)
        send(w.at[m, span, pc, q, pl.ds(0, 16), :], kind, m, light_up)
        send(w.at[m, span, pc, q, pl.ds(16, 16), :], kind, m, light_down)

    def prepare():
        wait(seg, misc_sem.at[1])
        wait(x.at[pl.ds(TAIL, TOK), :], misc_sem.at[0])
        pltpu.make_async_remote_copy(
            src_ref=x.at[pl.ds(TOK, TAIL), :], dst_ref=x.at[pl.ds(0, TAIL), :],
            send_sem=misc_sem.at[6], recv_sem=misc_sem.at[7],
            device_id=after, device_id_type=MESH,
        ).start()
        pltpu.make_async_remote_copy(
            src_ref=ids.at[:, pl.ds(TOK, 128)], dst_ref=ids.at[:, pl.ds(0, 128)],
            send_sem=misc_sem.at[8], recv_sem=misc_sem.at[9],
            device_id=after, device_id_type=MESH,
        ).start()

    def masks():
        wait(ck, misc_sem.at[2])
        wait(cb, misc_sem.at[3])
        wait(ng, misc_sem.at[4])
        wait(nb, misc_sem.at[5])

        def spread(u, _):
            lanes = pl.ds(pl.multiple_of(128 * u, 128), 128)
            for k in range(TAPS):
                taps[u, k] = jnp.broadcast_to(ckv[pl.ds(TAPS - 1 - k, 1), lanes], (8, 128))
            taps[u, TAPS] = jnp.broadcast_to(vecs[0, pl.ds(u, 1), :], (8, 128))
            return 0

        lax.fori_loop(0, 8, spread, 0)
        g[pl.ds(0, 8), :] = jnp.zeros((8, 128), F32)
        wait(ids.at[:, pl.ds(0, 128)], misc_sem.at[9])
        wait(x.at[pl.ds(0, TAIL), :], misc_sem.at[7])
        for b in range(5):
            row = ids[:, pl.ds(128 * b, 128)]
            if b == 0:
                row = jnp.where(sp == 0, -1, row)
            idc[pl.ds(128 * b, 128), :] = jnp.broadcast_to(row, (128, 128)).T

        def count(i, _):
            base = pl.multiple_of(8 * i, 8)
            here = idc[pl.ds(base + 96, 8), :]
            total = jnp.zeros((8, 128), jnp.int32)
            for k in range(1, TAPS):
                total = total + jnp.where(idc[pl.ds(base + 96 - k, 8), :] == here, 1, 0)
            dist[pl.ds(base, 8), :] = total
            return 0

        lax.fori_loop(0, ROWS // 8, count, 0)

    def compute(u):
        wu = w[u].reshape(2048, 256)
        half = ROWS // 2
        for i in range(2):
            r = jnp.dot(x[pl.ds(half * i, half), :], wu, preferred_element_type=F32)
            glu = r[:, :128] * jax.nn.sigmoid(r[:, 128:])
            g[pl.ds(8 + half * i, half), :] = glu.astype(BF16).astype(F32)

        def parts(i, wanted):
            base = pl.multiple_of(8 * i, 8)
            d = dist[pl.ds(base, 8), :]
            m = [g[pl.ds(base + 8, 8), :]]
            for j in range(1, 8):
                m.append(jnp.where(d >= j, g[pl.ds(base + 8 - j, 8), :], 0.0))
            sums = []
            for j in range(4):
                total = None
                if j in wanted:
                    for i8 in range(8):
                        if 8 * j + i8 < TAPS:
                            term = taps[u, 8 * j + i8] * m[i8]
                            total = term if total is None else total + term
                sums.append(total)
            return d, sums

        def step(i, carry):
            p1, p2, p3, q2, q3, r3 = carry
            results = []
            for s in range(4):
                d, (s0, s1, s2, s3) = parts(4 * i + s, (0, 1, 2, 3))
                total = taps[u, TAPS] + s0 + jnp.where(d >= 8, p1, 0.0)
                total = total + jnp.where(d >= 16, q2, 0.0) + jnp.where(d >= 24, r3, 0.0)
                results.append(total)
                p1, p2, p3, q2, q3, r3 = s1, s2, s3, p2, p3, q3
            base = pl.multiple_of(32 * i - TAIL, 32)
            conv[u, pl.ds(base, 32), :] = jnp.concatenate(results, axis=0).astype(BF16).astype(F32)
            return p1, p2, p3, q2, q3, r3

        _, (_, _, _, r3) = parts(1, (3,))
        _, (_, _, q2, q3) = parts(2, (2, 3))
        _, (_, p1, p2, p3) = parts(3, (1, 2, 3))
        lax.fori_loop(1, ROWS // 32, step, (p1, p2, p3, q2, q3, r3))

    def normalize():
        def step(i, _):
            rows = pl.ds(pl.multiple_of(64 * i, 64), 64)
            total = conv[0, rows, :]
            for u in range(1, 8):
                total = total + conv[u, rows, :]
            mean = jnp.sum(total, axis=1, keepdims=True) * (1.0 / 1024)
            square = None
            for u in range(8):
                off = conv[u, rows, :] - mean
                square = off * off if square is None else square + off * off
            var = jnp.sum(square, axis=1, keepdims=True) * (1.0 / 1024)
            scale = lax.rsqrt(var + 1e-05)
            for u in range(8):
                v = (conv[u, rows, :] - mean) * scale * vecs[1, pl.ds(u, 1), :] + vecs[2, pl.ds(u, 1), :]
                act[rows, pl.ds(128 * u, 128)] = (v * jax.nn.sigmoid(v)).astype(BF16)
            return 0

        lax.fori_loop(0, TOK // 64, step, 0)

    def slot(s, _):
        def stage(lead):
            m = s + lead
            return m, jnp.logical_and(m >= 0, m < UNITS)

        m0, on0 = stage(LEAD_SEND)

        @pl.when(on0)
        def _():
            wait(w.at[m0, 0, pc], load_sem.at[m0])
            own = w.at[m0, 0, pc, class_of(m0 % 2)]
            q = class_of(m0 % 2)
            for e, dy in ((2, 1), (1, -1), (4, 2), (3, -2)):
                send(own, 0, m0, at(dy=dy), w.at[m0, e, pc, q])
            send(w.at[m0, 0, pc], 4, m0, partner)

        @pl.when(s == 1 - LEAD_SEND)
        def _():
            prepare()

        m1, on1 = stage(LEAD_FORWARD)

        @pl.when(on1)
        def _():
            q = class_of(m1 % 2)
            wait(w.at[m1, pl.ds(1, 4), pc, q], recv_sem.at[0, m1])
            send(w.at[m1, 4, pc, q], 1, m1, at(dy=1), w.at[m1, 6, pc, q])
            send(w.at[m1, 3, pc, q], 1, m1, at(dy=-1), w.at[m1, 5, pc, q])
            low, high = pl.ds(0, 16), pl.ds(16, 16)
            send(w.at[m1, 4, pc, q, low, :], 1, m1, at(dy=2), w.at[m1, 7, pc, q, low, :])
            send(w.at[m1, 3, pc, q, high, :], 1, m1, at(dy=-2), w.at[m1, 7, pc, q, high, :])
            in_plane(m1, 1, 4, 2)

        m2, on2 = stage(LEAD_FAR)

        @pl.when(on2)
        def _():
            wait(w.at[m2, pl.ds(5, 3), pc, class_of(m2 % 2)], recv_sem.at[1, m2])
            in_plane(m2, 5, 3, 3)

        m3, on3 = stage(LEAD_NEAR_PAIR)

        @pl.when(on3)
        def _():
            wait(w.at[m3, pl.ds(1, 3), pc], recv_sem.at[2, m3])
            send(w.at[m3, pl.ds(1, 4), pc], 4, m3, partner)

        m4, on4 = stage(LEAD_FAR_PAIR)

        @pl.when(on4)
        def _():
            wait(w.at[m4, pl.ds(1, 3), pc, pl.ds(0, 3)], recv_sem.at[3, m4])
            send(w.at[m4, pl.ds(5, 3), pc], 4, m4, partner)

        @pl.when(s == -1)
        def _():
            masks()

        @pl.when(s >= 0)
        def _():
            wait(w.at[s, :, 1 - pc], recv_sem.at[4, s])

        @pl.when(jnp.logical_and(s >= 0, s < IN_UNITS))
        def _():
            compute(s)

        @pl.when(s == IN_UNITS - 1)
        def _():
            normalize()

        return 0

    lax.fori_loop(-LEAD_SEND, UNITS, slot, 0)

    def project(e, _):
        blocks = []
        for v in range(4):
            for h in range(2):
                lanes = pl.ds(128 * h, 128)
                blocks.append(jnp.concatenate(
                    [w[IN_UNITS + v, e, c, :, :, lanes].reshape(128, 128) for c in range(2)], axis=1))
        rhs = jnp.concatenate(blocks, axis=0)
        ost[e] = jnp.dot(act[...], rhs, preferred_element_type=F32).astype(BF16)
        dst = pl.multiple_of(256 * ((py + offset_of(e) + NY) % NY), 256)
        pltpu.make_async_copy(ost.at[e], out.at[:, pl.ds(dst, 256)], misc_sem.at[10]).start()
        return 0

    lax.fori_loop(0, 8, project, 0)

    wait(w.at[:, pl.ds(1, 4), 0, 0], send_sem.at[0])
    wait(w.at[:, pl.ds(5, 3), 0, 0], send_sem.at[1])
    wait(w.at[:, pl.ds(1, 3), 0], send_sem.at[2])
    wait(w.at[:, pl.ds(1, 3), 0, pl.ds(0, 3)], send_sem.at[3])
    wait(w.at[:, :, 0], send_sem.at[4])
    wait(x.at[pl.ds(0, TAIL), :], misc_sem.at[6])
    wait(ids.at[:, pl.ds(0, 128)], misc_sem.at[8])
    wait(ost, misc_sem.at[10])


def body(tokens, segments, w_lin, w_gate, w_out, conv_kernel, conv_bias, norm_gain, norm_bias):
    anywhere = pl.BlockSpec(memory_space=pl.ANY)
    result = pl.pallas_call(
        kernel,
        out_shape=jax.ShapeDtypeStruct((TOK, 2048), BF16),
        in_specs=[anywhere] * 9,
        out_specs=anywhere,
        scratch_shapes=[
            pltpu.VMEM((UNITS, 8, 2, 4, 32, 256), BF16),
            pltpu.VMEM((ROWS, 2048), BF16),
            pltpu.VMEM((1, 128 + TOK), jnp.int32),
            pltpu.VMEM((128 + TOK, 128), jnp.int32),
            pltpu.VMEM((ROWS, 128), jnp.int32),
            pltpu.VMEM((8, 32, 8, 128), F32),
            pltpu.VMEM((TAPS, 1024), F32),
            pltpu.VMEM((3, 8, 128), F32),
            pltpu.VMEM((8 + ROWS, 128), F32),
            pltpu.VMEM((8, TOK, 128), F32),
            pltpu.VMEM((TOK, 1024), BF16),
            pltpu.VMEM((8, TOK, 256), BF16),
            pltpu.SemaphoreType.DMA((UNITS,)),
            pltpu.SemaphoreType.DMA((11,)),
            pltpu.SemaphoreType.DMA((5, UNITS)),
            pltpu.SemaphoreType.DMA((5,)),
        ],
        compiler_params=pltpu.CompilerParams(
            collective_id=0, has_side_effects=True, vmem_limit_bytes=48 * 1024 * 1024
        ),
    )(
        tokens[0],
        segments,
        w_lin.reshape(4, 32, 1024),
        w_gate.reshape(4, 32, 1024),
        w_out.reshape(8, 4, 32, 128),
        conv_kernel,
        conv_bias.reshape(8, 128),
        norm_gain.reshape(8, 128),
        norm_bias.reshape(8, 128),
    )
    return result[None]


def solution(mesh):
    placed = (
        P("dp", "sp", None),
        P("dp", "sp"),
        P("dp", None),
        P("dp", None),
        P(None, "dp"),
        P(),
        P(),
        P(),
        P(),
    )
    return jax.shard_map(
        body, mesh=mesh, in_specs=placed, out_specs=P("dp", "sp", None), check_vma=False
    )
```

time: 141 us -> 83.1 us (0.59)
  waiting for transfers between devices: 83.4 us -> 0 us
  Pallas kernels: 0 us -> 73.3 us
  other arithmetic: 19.5 us -> 0 us
  matrix products: 13.5 us -> 0 us
  between operations: 13.5 us -> 0.02 us
  starting transfers between devices: 7.06 us -> 0 us
  local copies, waits for them, and re-layouts: 3.47 us -> 9.4 us
    all_gather x2 -> x0, waiting for transfers between devices: 81.4 us -> none  [the longest x1 55.9 us: sent_together(): result, at, outs = (lax.all_gather(both, axis, axis=dim, tiled=True), 0, [])]
    pallas_call x0 -> x1, Pallas kernels: none -> 73.3 us  [body(): pl.pallas_call(kernel, out_shape=jax.ShapeDtypeStruct((TOK, 2048), BF16),...]
    convert_element_type x1 -> x0, other arithmetic: 15.9 us -> none  [body(): conved = lax.optimization_barrier(conv.astype(jnp.bfloat16))]
    dot_general x3 -> x0, matrix products: 13.5 us -> none  [the longest x1 6.35 us: body(): jnp.einsum('ct,cr->tr', act, lax.all_gather(w_out, 'dp', axis=1, tiled=Tr...]
    unnamed x12 -> x19, local copies, waits for them, and re-layouts: 0.03 us -> 9.4 us
    ppermute x2 -> x0, starting transfers between devices: 7.01 us -> none  [from_behind(): return lax.ppermute(value, axis, pairs)]
    slice x5 -> x0, local copies, waits for them, and re-layouts: 3.32 us -> none  [the longest x1 1.37 us: conv_doc(): kernel[reach][:, None] * values[:, reach:].astype(jnp.float32)]
    concatenate x2 -> x0, other arithmetic: 2.1 us -> none  [the longest x1 2.02 us: sent_together(): both = jnp.concatenate(arrays, axis=along)]
  transfers between devices with their start and end apart: 4 -> 0, of which waited for: 3 -> 0; matrix products, arithmetic and copies ran while one was open for 20% -> 0% of each run, Pallas kernels for 0% -> 0%
where the time goes in v1:
time: 83.1 us; the launch traced here: 82.7 us
  Pallas kernels  73.3 us (88%)
  local copies, waits for them, and re-layouts  9.4 us (11%)
    pallas_call x1, Pallas kernels, body(): pl.pallas_call(kernel, out_shape=jax.ShapeDtypeStruct((TOK, 2048), BF16),...  73.3 us
    unnamed x19, local copies, waits for them, and re-layouts  9.4 us

profile of v1, /device:TPU:1, one launch (start us, length us, event | category | flops | bytes accessed | tf_op | source)
XLA Modules:
  0.0 82.7 jit_solution(15975476229712360532)
XLA Ops:
  0.0 0.0 copy-start
  0.0 1.6 %copy-done = bf16[1,512,2048]{2,1,0:T(8,128)(2,1)S(1)} copy-done((bf16[1,512,2048]{2,1,0:T(8,128)(2,1)S(1)}, bf16[1,512,2048]{2,1,0:T(8,128)(2,1)}, u32[]{:S(2)}) %copy-start) | copy-done | bytes 2097176
  1.6 0.0 copy-start.1
  1.6 0.9 %copy-done.1 = bf16[128,1024]{1,0:T(8,128)(2,1)S(1)} copy-done((bf16[128,1024]{1,0:T(8,128)(2,1)S(1)}, bf16[128,1024]{1,0:T(8,128)(2,1)}, u32[]{:S(2)}) %copy-start.1) | copy-done | bytes 262168
  2.5 0.0 copy-start.2
  2.5 0.9 %copy-done.2 = bf16[128,1024]{1,0:T(8,128)(2,1)S(1)} copy-done((bf16[128,1024]{1,0:T(8,128)(2,1)S(1)}, bf16[128,1024]{1,0:T(8,128)(2,1)}, u32[]{:S(2)}) %copy-start.2) | copy-done | bytes 262168
  3.5 0.0 copy-start.3
  3.5 0.9 %copy-done.3 = bf16[1024,128]{1,0:T(8,128)(2,1)S(1)} copy-done((bf16[1024,128]{1,0:T(8,128)(2,1)S(1)}, bf16[1024,128]{1,0:T(8,128)(2,1)}, u32[]{:S(2)}) %copy-start.3) | copy-done | bytes 262168
  4.4 0.0 copy-start.4
  4.4 0.9 %copy-done.4 = f32[31,1024]{1,0:T(8,128)S(1)} copy-done((f32[31,1024]{1,0:T(8,128)S(1)}, f32[31,1024]{1,0:T(8,128)}, u32[]{:S(2)}) %copy-start.4) | copy-done | bytes 127000
  5.3 0.0 copy-start.5
  5.4 0.7 copy-done.5
  6.0 0.0 copy-start.6
  6.0 0.7 copy-done.6
  6.7 0.0 copy-start.7
  6.7 0.7 copy-done.7
  7.4 0.0 copy-start.8
  7.4 0.7 copy-done.8
  8.1 73.3 %shard_map.91 = bf16[512,2048]{1,0:T(8,128)(2,1)S(1)} custom-call(bf16[512,2048]{1,0:T(8,128)(2,1)S(1)} %bitcast.9, s32[1,512]{1,0:T(1,128)S(1)} %copy-done.8, bf16[4,32,1024]{2,1,0:T(8,128)(2,1)S(1)} %bitcast.10, bf16[4,32,1024]{2,1,0:T(8,128)(2,1)S(1)} %bitcast.11, bf16[8,4,32,128]{3,2,1,0:T(8,128)(2,1)S(1)} %bitcast.12, f32[31,1024]{1,0:T(8,128)S(1)} %copy-done.4, ...), custom_call_target="tpu_custom_call" | custom-call | tf_op jit(solution)/shard_map/pallas_call | solution.py:309
  81.4 1.3 %copy.11 = bf16[1,512,2048]{2,1,0:T(8,128)(2,1)} copy(bf16[1,512,2048]{2,1,0:T(8,128)(2,1)S(1)} %bitcast.8) | data formatting | bytes 4194304
Async XLA Ops:
  0.0 1.6 %copy-start = (bf16[1,512,2048]{2,1,0:T(8,128)(2,1)S(1)}, bf16[1,512,2048]{2,1,0:T(8,128)(2,1)}, u32[]{:S(2)}) copy-start(bf16[1,512,2048]{2,1,0:T(8,128)(2,1)} %param.9) | copy-start | bytes 6291460
  1.6 0.9 %copy-start.1 = (bf16[128,1024]{1,0:T(8,128)(2,1)S(1)}, bf16[128,1024]{1,0:T(8,128)(2,1)}, u32[]{:S(2)}) copy-start(bf16[128,1024]{1,0:T(8,128)(2,1)} %param.11) | copy-start | bytes 786436
  2.5 0.9 %copy-start.2 = (bf16[128,1024]{1,0:T(8,128)(2,1)S(1)}, bf16[128,1024]{1,0:T(8,128)(2,1)}, u32[]{:S(2)}) copy-start(bf16[128,1024]{1,0:T(8,128)(2,1)} %param.12) | copy-start | bytes 786436
  3.5 0.9 %copy-start.3 = (bf16[1024,128]{1,0:T(8,128)(2,1)S(1)}, bf16[1024,128]{1,0:T(8,128)(2,1)}, u32[]{:S(2)}) copy-start(bf16[1024,128]{1,0:T(8,128)(2,1)} %param.13) | copy-start | bytes 786436
  4.4 0.9 %copy-start.4 = (f32[31,1024]{1,0:T(8,128)S(1)}, f32[31,1024]{1,0:T(8,128)}, u32[]{:S(2)}) copy-start(f32[31,1024]{1,0:T(8,128)} %ck.1) | copy-start | bytes 380932
  5.3 0.7 copy-start.5
  6.0 0.7 copy-start.6
  6.7 0.7 copy-start.7
  7.4 0.7 copy-start.8

commit v2 on v1

--- a/solution.py
+++ b/solution.py
@@ -13,7 +13,7 @@
 UNITS, IN_UNITS = 12, 8
 TOK, TAIL, ROWS = 512, 32, 544
 TAPS = 31
-LEAD_SEND, LEAD_FORWARD, LEAD_FAR, LEAD_NEAR_PAIR, LEAD_FAR_PAIR = 5, 3, 2, 2, 1
+LEAD_SEND, LEAD_FORWARD, LEAD_FAR, LEAD_NEAR_PAIR, LEAD_FAR_PAIR = 11, 8, 5, 5, 2
 
 
 def offset_of(e):
@@ -22,7 +22,7 @@
 
 def kernel(
     tok, seg, wl, wg, wo, ck, cb, ng, nb, out,
-    w, x, ids, idc, dist, taps, ckv, vecs, g, conv, act, ost,
+    w, x, ids, idc, dist, taps, ckv, vecs, g, conv, act,
     load_sem, misc_sem, recv_sem, send_sem,
 ):
     sp, dp = lax.axis_index("sp"), lax.axis_index("dp")
@@ -74,6 +74,23 @@
             device_id=peer, device_id_type=MESH,
         ).start()
 
+    def kind_of(m):
+        return 1 - (((m + 1) * 5) // UNITS - (m * 5) // UNITS)
+
+    for e in range(8):
+        src = pl.multiple_of(256 * ((py + offset_of(e) + NY) % NY), 256)
+        pltpu.make_async_remote_copy(
+            src_ref=tok.at[pl.ds(TOK - TAIL, TAIL), pl.ds(src, 256)],
+            dst_ref=x.at[pl.ds(0, TAIL), pl.ds(256 * e, 256)],
+            send_sem=misc_sem.at[6], recv_sem=misc_sem.at[7],
+            device_id=after, device_id_type=MESH,
+        ).start()
+    pltpu.make_async_remote_copy(
+        src_ref=seg.at[:, pl.ds(TOK - 128, 128)], dst_ref=ids.at[:, pl.ds(0, 128)],
+        send_sem=misc_sem.at[8], recv_sem=misc_sem.at[9],
+        device_id=after, device_id_type=MESH,
+    ).start()
+
     def class_of(parity):
         return (px * (1 + parity) + pz * (2 - parity)) % 4
 
@@ -84,7 +101,7 @@
                 mix(at(dz=1), at(dx=1)), mix(at(dz=-1), at(dx=-1)))
 
     def in_plane(m, first, count, kind):
-        parity = m % 2
+        parity = kind_of(m)
         q = class_of(parity)
         heavy_up, heavy_down, light_up, light_down = planes(parity)
         span = pl.ds(first, count)
@@ -94,21 +111,7 @@
         send(w.at[m, span, pc, q, pl.ds(0, 16), :], kind, m, light_up)
         send(w.at[m, span, pc, q, pl.ds(16, 16), :], kind, m, light_down)
 
-    def prepare():
-        wait(seg, misc_sem.at[1])
-        wait(x.at[pl.ds(TAIL, TOK), :], misc_sem.at[0])
-        pltpu.make_async_remote_copy(
-            src_ref=x.at[pl.ds(TOK, TAIL), :], dst_ref=x.at[pl.ds(0, TAIL), :],
-            send_sem=misc_sem.at[6], recv_sem=misc_sem.at[7],
-            device_id=after, device_id_type=MESH,
-        ).start()
-        pltpu.make_async_remote_copy(
-            src_ref=ids.at[:, pl.ds(TOK, 128)], dst_ref=ids.at[:, pl.ds(0, 128)],
-            send_sem=misc_sem.at[8], recv_sem=misc_sem.at[9],
-            device_id=after, device_id_type=MESH,
-        ).start()
-
-    def masks():
+    def spread_taps():
         wait(ck, misc_sem.at[2])
         wait(cb, misc_sem.at[3])
         wait(ng, misc_sem.at[4])
@@ -123,8 +126,10 @@
 
         lax.fori_loop(0, 8, spread, 0)
         g[pl.ds(0, 8), :] = jnp.zeros((8, 128), F32)
+
+    def masks():
+        wait(seg, misc_sem.at[1])
         wait(ids.at[:, pl.ds(0, 128)], misc_sem.at[9])
-        wait(x.at[pl.ds(0, TAIL), :], misc_sem.at[7])
         for b in range(5):
             row = ids[:, pl.ds(128 * b, 128)]
             if b == 0:
@@ -135,8 +140,8 @@
             base = pl.multiple_of(8 * i, 8)
             here = idc[pl.ds(base + 96, 8), :]
             total = jnp.zeros((8, 128), jnp.int32)
-            for k in range(1, TAPS):
-                total = total + jnp.where(idc[pl.ds(base + 96 - k, 8), :] == here, 1, 0)
+            for k, more in ((1, 1), (2, 1), (3, 1), (4, 1), (5, 1), (6, 1), (7, 1), (8, 1), (16, 8), (24, 8)):
+                total = total + jnp.where(idc[pl.ds(base + 96 - k, 8), :] == here, more, 0)
             dist[pl.ds(base, 8), :] = total
             return 0
 
@@ -147,47 +152,54 @@
         half = ROWS // 2
         for i in range(2):
             r = jnp.dot(x[pl.ds(half * i, half), :], wu, preferred_element_type=F32)
-            glu = r[:, :128] * jax.nn.sigmoid(r[:, 128:])
+            lin = 0.5 * r[:, :128]
+            glu = lin + lin * jnp.tanh(0.5 * r[:, 128:])
             g[pl.ds(8 + half * i, half), :] = glu.astype(BF16).astype(F32)
 
-        def parts(i, wanted):
+        def shifted(i):
             base = pl.multiple_of(8 * i, 8)
             d = dist[pl.ds(base, 8), :]
             m = [g[pl.ds(base + 8, 8), :]]
             for j in range(1, 8):
                 m.append(jnp.where(d >= j, g[pl.ds(base + 8 - j, 8), :], 0.0))
-            sums = []
-            for j in range(4):
-                total = None
-                if j in wanted:
-                    for i8 in range(8):
-                        if 8 * j + i8 < TAPS:
-                            term = taps[u, 8 * j + i8] * m[i8]
-                            total = term if total is None else total + term
-                sums.append(total)
-            return d, sums
+            return d, m
+
+        def sums(j, ms):
+            totals = [None] * len(ms)
+            for i8 in range(8):
+                if 8 * j + i8 < TAPS:
+                    tap = taps[u, 8 * j + i8]
+                    for n, m in enumerate(ms):
+                        term = tap * m[i8]
+                        totals[n] = term if totals[n] is None else totals[n] + term
+            return totals
 
         def step(i, carry):
             p1, p2, p3, q2, q3, r3 = carry
-            results = []
-            for s in range(4):
-                d, (s0, s1, s2, s3) = parts(4 * i + s, (0, 1, 2, 3))
-                total = taps[u, TAPS] + s0 + jnp.where(d >= 8, p1, 0.0)
-                total = total + jnp.where(d >= 16, q2, 0.0) + jnp.where(d >= 24, r3, 0.0)
-                results.append(total)
-                p1, p2, p3, q2, q3, r3 = s1, s2, s3, p2, p3, q3
+            ds, ms = zip(*[shifted(4 * i + n) for n in range(4)])
+            totals = [t + taps[u, TAPS] for t in sums(0, ms)]
+            s1 = [p1] + sums(1, ms)
+            totals = [t + jnp.where(d >= 8, p, 0.0) for t, d, p in zip(totals, ds, s1)]
+            s2 = [q2, p2] + sums(2, ms)
+            totals = [t + jnp.where(d >= 16, p, 0.0) for t, d, p in zip(totals, ds, s2)]
+            s3 = [r3, q3, p3] + sums(3, ms)
+            totals = [t + jnp.where(d >= 24, p, 0.0) for t, d, p in zip(totals, ds, s3)]
             base = pl.multiple_of(32 * i - TAIL, 32)
-            conv[u, pl.ds(base, 32), :] = jnp.concatenate(results, axis=0).astype(BF16).astype(F32)
-            return p1, p2, p3, q2, q3, r3
-
-        _, (_, _, _, r3) = parts(1, (3,))
-        _, (_, _, q2, q3) = parts(2, (2, 3))
-        _, (_, p1, p2, p3) = parts(3, (1, 2, 3))
+            for n in range(4):
+                conv[u, pl.ds(base + 8 * n, 8), :] = totals[n].astype(BF16).astype(F32)
+            return s1[4], s2[5], s3[6], s2[4], s3[5], s3[4]
+
+        _, m1 = shifted(1)
+        _, m2 = shifted(2)
+        _, m3 = shifted(3)
+        p1 = sums(1, [m3])[0]
+        q2, p2 = sums(2, [m2, m3])
+        r3, q3, p3 = sums(3, [m1, m2, m3])
         lax.fori_loop(1, ROWS // 32, step, (p1, p2, p3, q2, q3, r3))
 
     def normalize():
         def step(i, _):
-            rows = pl.ds(pl.multiple_of(64 * i, 64), 64)
+            rows = pl.ds(pl.multiple_of(128 * i, 128), 128)
             total = conv[0, rows, :]
             for u in range(1, 8):
                 total = total + conv[u, rows, :]
@@ -200,12 +212,15 @@
             scale = lax.rsqrt(var + 1e-05)
             for u in range(8):
                 v = (conv[u, rows, :] - mean) * scale * vecs[1, pl.ds(u, 1), :] + vecs[2, pl.ds(u, 1), :]
-                act[rows, pl.ds(128 * u, 128)] = (v * jax.nn.sigmoid(v)).astype(BF16)
+                half = 0.5 * v
+                act[rows, pl.ds(128 * u, 128)] = (half + half * jnp.tanh(half)).astype(BF16)
             return 0
 
-        lax.fori_loop(0, TOK // 64, step, 0)
-
-    def slot(s, _):
+        lax.fori_loop(0, TOK // 128, step, 0)
+
+    def slot(t, _):
+        s = t - LEAD_SEND
+
         def stage(lead):
             m = s + lead
             return m, jnp.logical_and(m >= 0, m < UNITS)
@@ -215,21 +230,21 @@
         @pl.when(on0)
         def _():
             wait(w.at[m0, 0, pc], load_sem.at[m0])
-            own = w.at[m0, 0, pc, class_of(m0 % 2)]
-            q = class_of(m0 % 2)
+            own = w.at[m0, 0, pc, class_of(kind_of(m0))]
+            q = class_of(kind_of(m0))
             for e, dy in ((2, 1), (1, -1), (4, 2), (3, -2)):
                 send(own, 0, m0, at(dy=dy), w.at[m0, e, pc, q])
             send(w.at[m0, 0, pc], 4, m0, partner)
 
-        @pl.when(s == 1 - LEAD_SEND)
-        def _():
-            prepare()
+        @pl.when(s == -LEAD_FORWARD)
+        def _():
+            spread_taps()
 
         m1, on1 = stage(LEAD_FORWARD)
 
         @pl.when(on1)
         def _():
-            q = class_of(m1 % 2)
+            q = class_of(kind_of(m1))
             wait(w.at[m1, pl.ds(1, 4), pc, q], recv_sem.at[0, m1])
             send(w.at[m1, 4, pc, q], 1, m1, at(dy=1), w.at[m1, 6, pc, q])
             send(w.at[m1, 3, pc, q], 1, m1, at(dy=-1), w.at[m1, 5, pc, q])
@@ -242,7 +257,7 @@
 
         @pl.when(on2)
         def _():
-            wait(w.at[m2, pl.ds(5, 3), pc, class_of(m2 % 2)], recv_sem.at[1, m2])
+            wait(w.at[m2, pl.ds(5, 3), pc, class_of(kind_of(m2))], recv_sem.at[1, m2])
             in_plane(m2, 5, 3, 3)
 
         m3, on3 = stage(LEAD_NEAR_PAIR)
@@ -257,18 +272,21 @@
         @pl.when(on4)
         def _():
             wait(w.at[m4, pl.ds(1, 3), pc, pl.ds(0, 3)], recv_sem.at[3, m4])
-            send(w.at[m4, pl.ds(5, 3), pc], 4, m4, partner)
-
-        @pl.when(s == -1)
+            send(w.at[m4, pl.ds(5, 3), pc], 5, m4, partner)
+
+        @pl.when(s == 1 - LEAD_FORWARD)
         def _():
             masks()
 
-        @pl.when(s >= 0)
-        def _():
-            wait(w.at[s, :, 1 - pc], recv_sem.at[4, s])
+        @pl.when(s == 0)
+        def _():
+            wait(x.at[pl.ds(TAIL, TOK), :], misc_sem.at[0])
+            wait(x.at[pl.ds(0, TAIL), :], misc_sem.at[7])
 
         @pl.when(jnp.logical_and(s >= 0, s < IN_UNITS))
         def _():
+            wait(w.at[s, pl.ds(0, 5), 1 - pc], recv_sem.at[4, s])
+            wait(w.at[s, pl.ds(5, 3), 1 - pc], recv_sem.at[5, s])
             compute(s)
 
         @pl.when(s == IN_UNITS - 1)
@@ -277,40 +295,49 @@
 
         return 0
 
-    lax.fori_loop(-LEAD_SEND, UNITS, slot, 0)
-
-    def project(e, _):
+    lax.fori_loop(0, UNITS - LEAD_FAR_PAIR + LEAD_SEND, slot, 0)
+
+    def rhs_of(e):
         blocks = []
         for v in range(4):
             for h in range(2):
                 lanes = pl.ds(128 * h, 128)
                 blocks.append(jnp.concatenate(
                     [w[IN_UNITS + v, e, c, :, :, lanes].reshape(128, 128) for c in range(2)], axis=1))
-        rhs = jnp.concatenate(blocks, axis=0)
-        ost[e] = jnp.dot(act[...], rhs, preferred_element_type=F32).astype(BF16)
-        dst = pl.multiple_of(256 * ((py + offset_of(e) + NY) % NY), 256)
-        pltpu.make_async_copy(ost.at[e], out.at[:, pl.ds(dst, 256)], misc_sem.at[10]).start()
+        return jnp.concatenate(blocks, axis=0)
+
+    def project(i, _):
+        pair = (2 * i, 2 * i + 1)
+        rhs = jnp.concatenate([rhs_of(e) for e in pair], axis=1)
+        both = jnp.dot(act[...], rhs, preferred_element_type=F32).astype(BF16)
+        for n, e in enumerate(pair):
+            dst = pl.multiple_of(256 * ((py + offset_of(e) + NY) % NY), 256)
+            out[:, pl.ds(dst, 256)] = both[:, 256 * n : 256 * (n + 1)]
         return 0
 
-    lax.fori_loop(0, 8, project, 0)
+    for v in range(IN_UNITS, UNITS):
+        wait(w.at[v, pl.ds(0, 5), 1 - pc], recv_sem.at[4, v])
+    lax.fori_loop(0, 2, project, 0)
+    for v in range(IN_UNITS, UNITS):
+        wait(w.at[v, pl.ds(5, 3), 1 - pc], recv_sem.at[5, v])
+    lax.fori_loop(2, 4, project, 0)
 
     wait(w.at[:, pl.ds(1, 4), 0, 0], send_sem.at[0])
     wait(w.at[:, pl.ds(5, 3), 0, 0], send_sem.at[1])
     wait(w.at[:, pl.ds(1, 3), 0], send_sem.at[2])
     wait(w.at[:, pl.ds(1, 3), 0, pl.ds(0, 3)], send_sem.at[3])
-    wait(w.at[:, :, 0], send_sem.at[4])
+    wait(w.at[:, pl.ds(0, 5), 0], send_sem.at[4])
+    wait(w.at[:, pl.ds(5, 3), 0], send_sem.at[5])
     wait(x.at[pl.ds(0, TAIL), :], misc_sem.at[6])
     wait(ids.at[:, pl.ds(0, 128)], misc_sem.at[8])
-    wait(ost, misc_sem.at[10])
 
 
 def body(tokens, segments, w_lin, w_gate, w_out, conv_kernel, conv_bias, norm_gain, norm_bias):
-    anywhere = pl.BlockSpec(memory_space=pl.ANY)
     result = pl.pallas_call(
         kernel,
         out_shape=jax.ShapeDtypeStruct((TOK, 2048), BF16),
-        in_specs=[anywhere] * 9,
-        out_specs=anywhere,
+        in_specs=[pl.BlockSpec(memory_space=pltpu.HBM)] * 9,
+        out_specs=pl.BlockSpec(memory_space=pltpu.VMEM),
         scratch_shapes=[
             pltpu.VMEM((UNITS, 8, 2, 4, 32, 256), BF16),
             pltpu.VMEM((ROWS, 2048), BF16),
@@ -323,16 +350,16 @@
             pltpu.VMEM((8 + ROWS, 128), F32),
             pltpu.VMEM((8, TOK, 128), F32),
             pltpu.VMEM((TOK, 1024), BF16),
-            pltpu.VMEM((8, TOK, 256), BF16),
             pltpu.SemaphoreType.DMA((UNITS,)),
-            pltpu.SemaphoreType.DMA((11,)),
-            pltpu.SemaphoreType.DMA((5, UNITS)),
-            pltpu.SemaphoreType.DMA((5,)),
+            pltpu.SemaphoreType.DMA((10,)),
+            pltpu.SemaphoreType.DMA((6, UNITS)),
+            pltpu.SemaphoreType.DMA((6,)),
         ],
         compiler_params=pltpu.CompilerParams(
-            collective_id=0, has_side_effects=True, vmem_limit_bytes=48 * 1024 * 1024
+            collective_id=0, has_side_effects=True, vmem_limit_bytes=40 * 1024 * 1024
         ),
     )(
+        *[pltpu.with_memory_space_constraint(a, pltpu.HBM) for a in (
         tokens[0],
         segments,
         w_lin.reshape(4, 32, 1024),
@@ -342,6 +369,7 @@
         conv_bias.reshape(8, 128),
         norm_gain.reshape(8, 128),
         norm_bias.reshape(8, 128),
+        )]
     )
     return result[None]
 

time: 83.1 us -> 54.4 us (0.65)
  Pallas kernels: 73.3 us -> 53 us
  local copies, waits for them, and re-layouts: 9.4 us -> 1.32 us
    pallas_call x1, Pallas kernels: 73.3 us -> 53 us  [body(): pl.pallas_call(kernel, out_shape=jax.ShapeDtypeStruct((TOK, 2048), BF16),...]
    unnamed x19 -> x1, local copies, waits for them, and re-layouts: 9.4 us -> 1.32 us
where the time goes in v2:
time: 54.4 us; the launch traced here: 54.3 us
  Pallas kernels  53 us (97%)
  local copies, waits for them, and re-layouts  1.32 us (2%)
    pallas_call x1, Pallas kernels, body(): pl.pallas_call(kernel, out_shape=jax.ShapeDtypeStruct((TOK, 2048), BF16),...  53 us
    unnamed x1, local copies, waits for them, and re-layouts  1.32 us

profile of v2, /device:TPU:1, one launch (start us, length us, event | category | flops | bytes accessed | tf_op | source)
XLA Modules:
  0.0 54.3 jit_solution(11543606683696072347)
XLA Ops:
  0.0 53.0 %shard_map.91 = bf16[512,2048]{1,0:T(8,128)(2,1)S(1)} custom-call(bf16[512,2048]{1,0:T(8,128)(2,1)} %bitcast.9, s32[1,512]{1,0:T(1,128)} %seg.1, bf16[4,32,1024]{2,1,0:T(8,128)(2,1)} %bitcast.10, bf16[4,32,1024]{2,1,0:T(8,128)(2,1)} %bitcast.11, bf16[8,4,32,128]{3,2,1,0:T(8,128)(2,1)} %bitcast.12, f32[31,1024]{1,0:T(8,128)} %ck.1, f32[8,128]{1,0:T(8,128)} %bitcast.13, ...), custom_call_target="tpu_custom_call" | custom-call | tf_op jit(solution)/shard_map/pallas_call | solution.py:336
  53.0 1.3 %copy.11 = bf16[1,512,2048]{2,1,0:T(8,128)(2,1)} copy(bf16[1,512,2048]{2,1,0:T(8,128)(2,1)S(1)} %bitcast.8) | data formatting | bytes 4194304

commit v3 on v2

--- a/solution.py
+++ b/solution.py
@@ -13,7 +13,7 @@
 UNITS, IN_UNITS = 12, 8
 TOK, TAIL, ROWS = 512, 32, 544
 TAPS = 31
-LEAD_SEND, LEAD_FORWARD, LEAD_FAR, LEAD_NEAR_PAIR, LEAD_FAR_PAIR = 11, 8, 5, 5, 2
+LEAD_SEND, LEAD_FORWARD, LEAD_FAR, LEAD_NEAR_PAIR, LEAD_FAR_PAIR = 12, 8, 5, 5, 2
 
 
 def offset_of(e):
@@ -289,10 +289,6 @@
             wait(w.at[s, pl.ds(5, 3), 1 - pc], recv_sem.at[5, s])
             compute(s)
 
-        @pl.when(s == IN_UNITS - 1)
-        def _():
-            normalize()
-
         return 0
 
     lax.fori_loop(0, UNITS - LEAD_FAR_PAIR + LEAD_SEND, slot, 0)
@@ -315,6 +311,7 @@
             out[:, pl.ds(dst, 256)] = both[:, 256 * n : 256 * (n + 1)]
         return 0
 
+    normalize()
     for v in range(IN_UNITS, UNITS):
         wait(w.at[v, pl.ds(0, 5), 1 - pc], recv_sem.at[4, v])
     lax.fori_loop(0, 2, project, 0)

time: 54.4 us -> 53 us (0.974)
  Pallas kernels: 53 us -> 51.5 us
    pallas_call x1, Pallas kernels: 53 us -> 51.5 us  [body(): pl.pallas_call(kernel, out_shape=jax.ShapeDtypeStruct((TOK, 2048), BF16),...]
where the time goes in v3:
time: 53 us; the launch traced here: 52.9 us
  Pallas kernels  51.5 us (97%)
  local copies, waits for them, and re-layouts  1.32 us (2%)
    pallas_call x1, Pallas kernels, body(): pl.pallas_call(kernel, out_shape=jax.ShapeDtypeStruct((TOK, 2048), BF16),...  51.5 us
    unnamed x1, local copies, waits for them, and re-layouts  1.32 us

profile of v3, /device:TPU:1, one launch (start us, length us, event | category | flops | bytes accessed | tf_op | source)
XLA Modules:
  0.0 52.9 jit_solution(3007278492350593189)
XLA Ops:
  0.0 51.5 %shard_map.91 = bf16[512,2048]{1,0:T(8,128)(2,1)S(1)} custom-call(bf16[512,2048]{1,0:T(8,128)(2,1)} %bitcast.9, s32[1,512]{1,0:T(1,128)} %seg.1, bf16[4,32,1024]{2,1,0:T(8,128)(2,1)} %bitcast.10, bf16[4,32,1024]{2,1,0:T(8,128)(2,1)} %bitcast.11, bf16[8,4,32,128]{3,2,1,0:T(8,128)(2,1)} %bitcast.12, f32[31,1024]{1,0:T(8,128)} %ck.1, f32[8,128]{1,0:T(8,128)} %bitcast.13, ...), custom_call_target="tpu_custom_call" | custom-call | tf_op jit(solution)/shard_map/pallas_call | solution.py:333
  51.5 1.3 %copy.11 = bf16[1,512,2048]{2,1,0:T(8,128)(2,1)} copy(bf16[1,512,2048]{2,1,0:T(8,128)(2,1)S(1)} %bitcast.8) | data formatting | bytes 4194304

commit v4 on v3

--- a/solution.py
+++ b/solution.py
@@ -147,7 +147,7 @@
 
         lax.fori_loop(0, ROWS // 8, count, 0)
 
-    def compute(u):
+    def gate_unit(u):
         wu = w[u].reshape(2048, 256)
         half = ROWS // 2
         for i in range(2):
@@ -156,6 +156,7 @@
             glu = lin + lin * jnp.tanh(0.5 * r[:, 128:])
             g[pl.ds(8 + half * i, half), :] = glu.astype(BF16).astype(F32)
 
+    def convolve(u):
         def shifted(i):
             base = pl.multiple_of(8 * i, 8)
             d = dist[pl.ds(base, 8), :]
@@ -253,6 +254,17 @@
             send(w.at[m1, 3, pc, q, high, :], 1, m1, at(dy=-2), w.at[m1, 7, pc, q, high, :])
             in_plane(m1, 1, 4, 2)
 
+        @pl.when(s == 0)
+        def _():
+            wait(x.at[pl.ds(TAIL, TOK), :], misc_sem.at[0])
+            wait(x.at[pl.ds(0, TAIL), :], misc_sem.at[7])
+
+        @pl.when(jnp.logical_and(s >= 0, s < IN_UNITS))
+        def _():
+            wait(w.at[s, pl.ds(0, 5), 1 - pc], recv_sem.at[4, s])
+            wait(w.at[s, pl.ds(5, 3), 1 - pc], recv_sem.at[5, s])
+            gate_unit(s)
+
         m2, on2 = stage(LEAD_FAR)
 
         @pl.when(on2)
@@ -278,16 +290,9 @@
         def _():
             masks()
 
-        @pl.when(s == 0)
-        def _():
-            wait(x.at[pl.ds(TAIL, TOK), :], misc_sem.at[0])
-            wait(x.at[pl.ds(0, TAIL), :], misc_sem.at[7])
-
         @pl.when(jnp.logical_and(s >= 0, s < IN_UNITS))
         def _():
-            wait(w.at[s, pl.ds(0, 5), 1 - pc], recv_sem.at[4, s])
-            wait(w.at[s, pl.ds(5, 3), 1 - pc], recv_sem.at[5, s])
-            compute(s)
+            convolve(s)
 
         return 0
 

time: 53 us -> 53.1 us (level)
  no operation moved by 1% of the time
where the time goes in v4:
time: 53.1 us; the launch traced here: 53 us
  Pallas kernels  51.6 us (97%)
  local copies, waits for them, and re-layouts  1.32 us (2%)
    pallas_call x1, Pallas kernels, body(): pl.pallas_call(kernel, out_shape=jax.ShapeDtypeStruct((TOK, 2048), BF16),...  51.6 us
    unnamed x1, local copies, waits for them, and re-layouts  1.32 us

profile of v4, /device:TPU:1, one launch (start us, length us, event | category | flops | bytes accessed | tf_op | source)
XLA Modules:
  0.0 53.0 jit_solution(17915572075696105919)
XLA Ops:
  0.0 51.6 %shard_map.91 = bf16[512,2048]{1,0:T(8,128)(2,1)S(1)} custom-call(bf16[512,2048]{1,0:T(8,128)(2,1)} %bitcast.9, s32[1,512]{1,0:T(1,128)} %seg.1, bf16[4,32,1024]{2,1,0:T(8,128)(2,1)} %bitcast.10, bf16[4,32,1024]{2,1,0:T(8,128)(2,1)} %bitcast.11, bf16[8,4,32,128]{3,2,1,0:T(8,128)(2,1)} %bitcast.12, f32[31,1024]{1,0:T(8,128)} %ck.1, f32[8,128]{1,0:T(8,128)} %bitcast.13, ...), custom_call_target="tpu_custom_call" | custom-call | tf_op jit(solution)/shard_map/pallas_call | solution.py:338
  51.6 1.3 %copy.11 = bf16[1,512,2048]{2,1,0:T(8,128)(2,1)} copy(bf16[1,512,2048]{2,1,0:T(8,128)(2,1)S(1)} %bitcast.8) | data formatting | bytes 4194304
